TPU v7x, 256 devices: a 8x8x2 block of a 8x8x16 slice. The times are simulated.
256 devices in a mesh: grp: 2 (over z), kv: 16 (over y, core), tp: 8 (over x).
Axes of the slice: x: 8, y: 8, z: 2, core: 2. Of those that a mesh axis runs over, the one named last changes fastest.
The devices are a block of a 8x8x16 slice.
Arguments:
- tokens: bfloat16 [512, 4096], P('grp', ('kv', 'tp')), parts along dimension 0, may hold values from -20 to 20, as said below
- norm_gain: bfloat16 [4096], P('kv'), may hold values from 0.099609375 to 1.8984375
- w_query: bfloat16 [4096, 2048], P('kv', 'tp'), may hold values from -0.09375 to 0.09375
- w_key: bfloat16 [4096, 2048], P('kv', 'tp'), may hold values from -0.09375 to 0.09375
- w_value: bfloat16 [4096, 4096], P('kv', 'tp'), may hold values from -0.09375 to 0.09375
- w_outgate: bfloat16 [4096, 4096], P('kv', 'tp'), may hold values from -0.09375 to 0.09375
- w_input_gate: bfloat16 [4096, 32], P('kv'), may hold values from -0.09375 to 0.09375
- w_forget_gate: bfloat16 [4096, 32], P('kv'), may hold values from -0.09375 to 0.09375
- memory: float32 [512, 32, 64, 128], P(('grp', 'kv'), 'tp'), parts along dimension 0, may hold values from -4 to 4
- normalizer: float32 [512, 32, 64], P(('grp', 'kv'), 'tp'), parts along dimension 0, may hold values from -4 to 4
- stabilizer: float32 [512, 32], P(('grp', 'kv'), 'tp'), parts along dimension 0, may hold values from -4 to 4
- w_mix_out: bfloat16 [4096, 4096], P('tp', 'kv'), may hold values from -0.09375 to 0.09375
- ffn_gain: bfloat16 [4096], P('kv'), may hold values from 0.099609375 to 1.8984375
- w_gate: bfloat16 [4096, 11264], P('kv', 'tp'), may hold values from -0.09375 to 0.09375
- w_up: bfloat16 [4096, 11264], P('kv', 'tp'), may hold values from -0.09375 to 0.09375
- w_down: bfloat16 [11264, 4096], P('tp', 'kv'), may hold values from -0.3125 to 0.3125
Outputs:
- layer_out: bfloat16 [512, 4096], P('grp', ('kv', 'tp')), parts along dimension 0
- new_memory: float32 [512, 32, 64, 128], P(('grp', 'kv'), 'tp'), parts along dimension 0
- new_normalizer: float32 [512, 32, 64], P(('grp', 'kv'), 'tp'), parts along dimension 0
- new_stabilizer: float32 [512, 32], P(('grp', 'kv'), 'tp'), parts along dimension 0
There are 2 independent parts, one for each index of `grp`. A program takes and returns all parts, laid end to end along the dimension named above; an argument that names none is the same for every part. Nothing has to cross between parts.
Inputs may be any that keep to these rules, and one draw needn't show every extreme that they name: tokens' feature scales differ by column and by sequence.
All inputs are finite; a program needn't handle non-finite values.
Results may differ from a plain program's by a relative error of at most 0.029.
Values may be sent and summed in bfloat16 or wider, within the bound.
No kernel may reach another device: no remote copies, remote signals or barrier semaphores. Data moves between devices by JAX's collectives and lax.ppermute only.
A program may use at most 64 MiB of HBM per device.

v0:
```python
import jax
import jax.numpy as jnp
from jax import lax
from jax.sharding import PartitionSpec as P

D = 4096
DQK = 64
DV = 128


def copy_for_each(array, axis):
    count = lax.axis_size(axis)
    return lax.all_to_all(
        jnp.broadcast_to(array[None], (count, *array.shape)), axis, 0, 0, tiled=True
    )


def laid_out(pieces, dim):
    lengths = list(pieces.shape[1:])
    lengths[dim] *= pieces.shape[0]
    return jnp.moveaxis(pieces, 0, dim).reshape(lengths)


def gather_directly(array, axis, dim):
    pieces = copy_for_each(array, axis)
    return laid_out(pieces, dim)


def split_up(array, dim, count):
    before, after = (array.shape[:dim], array.shape[dim + 1 :])
    return jnp.moveaxis(array.reshape(*before, count, -1, *after), dim, 0)


def summed_on_arrival(array, axis, dim):
    count = lax.axis_size(axis)
    pieces = lax.all_to_all(split_up(array, dim, count), axis, 0, 0, tiled=True)
    return jnp.sum(pieces, axis=0)


def sum_at_owner(array, axis, dim):
    count = lax.axis_size(axis)
    pieces = lax.all_to_all(split_up(array, dim, count), axis, 0, 0, tiled=True)
    return jnp.sum(pieces.astype(jnp.float32), axis=0)


def in_one_piece(arrays, axis, dim, along):
    ends, at = ([], 0)
    for a in arrays[:-1]:
        at += a.shape[along]
        ends.append(at)
    both = jnp.concatenate(arrays, axis=along)
    return tuple(
        jnp.split(lax.psum_scatter(both, axis, scatter_dimension=dim, tiled=True), ends, axis=along)
    )


def over_copies(array, axis):
    return copy_for_each(array, axis).sum(axis=0)


def shards(
    tokens,
    norm_gain,
    w_query,
    w_key,
    w_value,
    w_outgate,
    w_input_gate,
    w_forget_gate,
    memory,
    normalizer,
    stabilizer,
    w_mix_out,
    ffn_gain,
    w_gate,
    w_up,
    w_down,
):
    seqs = tokens.shape[0]
    weights = (w_query, w_key, w_value, w_outgate, w_input_gate, w_forget_gate)
    start_proj = tuple((jnp.zeros((seqs, weight.shape[1]), jnp.float32) for weight in weights))
    start_proj = start_proj + (jnp.zeros((seqs,), jnp.float32),)
    wide = gather_directly(tokens, "tp", 1).astype(jnp.float32)
    gain = norm_gain.astype(jnp.float32)
    normed = (wide * gain[None, :]).astype(jnp.bfloat16)
    sums = tuple(
        (jnp.dot(normed, weight, preferred_element_type=jnp.float32) for weight in weights)
    )
    totals = sums + (jnp.sum(wide * wide, axis=1),)
    z_query, z_key, z_value, z_outgate, z_input, z_forget, squares = jax.tree.map(
        lambda part: summed_on_arrival(part, "kv", 0), totals
    )
    own = z_query.shape[0]
    local_heads = memory.shape[1]
    scale1 = lax.rsqrt(squares / D + 1e-06)
    head_start = lax.axis_index("tp") * local_heads
    query = (scale1[:, None] * z_query).reshape(own, local_heads, DQK) * DQK ** (-0.5)
    key = (scale1[:, None] * z_key).reshape(own, local_heads, DQK)
    value = (scale1[:, None] * z_value).reshape(own, local_heads, DV)
    outgate = scale1[:, None] * z_outgate
    igate = scale1[:, None] * lax.dynamic_slice_in_dim(z_input, head_start, local_heads, 1)
    lforget = jax.nn.log_sigmoid(
        scale1[:, None] * lax.dynamic_slice_in_dim(z_forget, head_start, local_heads, 1)
    )
    new_stabilizer = jnp.maximum(lforget + stabilizer, igate)
    decay = jnp.exp(lforget + stabilizer - new_stabilizer)
    inflow = jnp.exp(igate - new_stabilizer)
    new_memory = (
        decay[:, :, None, None] * memory
        + inflow[:, :, None, None] * key[:, :, :, None] * value[:, :, None, :]
    )
    new_normalizer = decay[:, :, None] * normalizer + inflow[:, :, None] * key
    numer = jnp.einsum("bhd,bhde->bhe", query, new_memory)
    denom = jnp.sum(query * new_normalizer, axis=-1)
    readout = numer / jnp.maximum(jnp.abs(denom), jnp.exp(-new_stabilizer))[:, :, None]
    gated = (jax.nn.sigmoid(outgate) * readout.reshape(own, local_heads * DV)).astype(jnp.bfloat16)
    mix_partial = jnp.dot(
        gather_directly(gated, "kv", 0), w_mix_out, preferred_element_type=jnp.float32
    )
    mix_total = sum_at_owner(mix_partial.astype(jnp.bfloat16), "tp", 1)
    mixed_in = (tokens.astype(jnp.float32) + mix_total).astype(jnp.bfloat16)
    wide = gather_directly(mixed_in, "tp", 1).astype(jnp.float32)
    gain = ffn_gain.astype(jnp.float32)
    normed = (wide * gain[None, :]).astype(jnp.bfloat16)
    gate_sum = jnp.dot(normed, w_gate, preferred_element_type=jnp.float32)
    up_sum = jnp.dot(normed, w_up, preferred_element_type=jnp.float32)
    square_part = jnp.sum(wide * wide, axis=1)
    gate_share, up_share = in_one_piece((gate_sum, up_sum), "kv", 1, 0)
    square_sum = over_copies(square_part, "kv")
    scale2 = lax.rsqrt(square_sum / D + 1e-06)[:, None]
    hidden_share = (jax.nn.silu(scale2 * gate_share) * (scale2 * up_share)).astype(jnp.bfloat16)
    down_partial = jnp.dot(
        lax.all_gather(hidden_share, "kv", axis=1, tiled=True),
        w_down,
        preferred_element_type=jnp.float32,
    )
    down_total = sum_at_owner(down_partial.astype(jnp.bfloat16), "tp", 1)
    layer_out = (mixed_in.astype(jnp.float32) + down_total).astype(jnp.bfloat16)
    return (layer_out, new_memory, new_normalizer, new_stabilizer)


def solution(mesh):
    in_specs = (
        P("grp", ("kv", "tp")),
        P("kv"),
        P("kv", "tp"),
        P("kv", "tp"),
        P("kv", "tp"),
        P("kv", "tp"),
        P("kv", None),
        P("kv", None),
        P(("grp", "kv"), "tp", None, None),
        P(("grp", "kv"), "tp", None),
        P(("grp", "kv"), "tp"),
        P("tp", "kv"),
        P("kv"),
        P("kv", "tp"),
        P("kv", "tp"),
        P("tp", "kv"),
    )
    out_specs = (
        P("grp", ("kv", "tp")),
        P(("grp", "kv"), "tp", None, None),
        P(("grp", "kv"), "tp", None),
        P(("grp", "kv"), "tp"),
    )
    return jax.shard_map(shards, mesh=mesh, in_specs=in_specs, out_specs=out_specs, check_vma=False)
```

profile of v0, /device:TPU:513, one launch (start us, length us, event | category | flops | bytes accessed | tf_op | source)
XLA Modules:
  0.0 294.8 jit_solution(17293236000279843596)
XLA Ops:
  8.7 7.9 %all-to-all-start = ((bf16[8,256,32]{1,2,0:T(8,128)(2,1)}), bf16[8,256,32]{1,2,0:T(8,128)(2,1)S(1)}, u32[]{:S(2)}, u32[]{:S(2)}) async-start(bf16[8,256,32]{1,2,0:T(8,128)(2,1)} %broadcast_in_dim.8), calls=%async_computation | async-start | bytes 262144 | tf_op jit(solution)/shard_map/all_to_all | solution.py:13
  17.2 7.3 %all-to-all-done = bf16[8,256,32]{1,2,0:T(8,128)(2,1)S(1)} async-done(((bf16[8,256,32]{1,2,0:T(8,128)(2,1)}), bf16[8,256,32]{1,2,0:T(8,128)(2,1)S(1)}, u32[]{:S(2)}, u32[]{:S(2)}) %all-to-all-start) | async-done | bytes 131104 | tf_op jit(solution)/shard_map/all_to_all | solution.py:13
  25.2 20.3 %all-to-all-start.1 = ((f32[16,1,16]{2,1,0:T(1,128)}), f32[16,1,16]{2,1,0:T(1,128)S(1)}, u32[]{:S(2)}, u32[]{:S(2)}) async-start(f32[16,1,16]{2,1,0:T(1,128)} %all_to_all.44), calls=%async_computation.1 | async-start | bytes 16384 | tf_op jit(solution)/shard_map/all_to_all | solution.py:36
  47.3 5.3 %all-to-all-done.1 = f32[16,1,16]{2,1,0:T(1,128)S(1)} async-done(((f32[16,1,16]{2,1,0:T(1,128)}), f32[16,1,16]{2,1,0:T(1,128)S(1)}, u32[]{:S(2)}, u32[]{:S(2)}) %all-to-all-start.1) | async-done | bytes 1056 | tf_op jit(solution)/shard_map/all_to_all | solution.py:36
  52.6 4.0 %all-to-all-start.5 = ((f32[16,1,512]{2,1,0:T(1,128)}), f32[16,1,512]{2,1,0:T(1,128)S(1)}, u32[]{:S(2)}, u32[]{:S(2)}) async-start(f32[16,1,512]{2,1,0:T(1,128)} %reshape.179), calls=%async_computation.5 | async-start | bytes 65536 | tf_op jit(solution)/shard_map/all_to_all | solution.py:36
  57.5 6.7 %all-to-all-done.5 = f32[16,1,512]{2,1,0:T(1,128)S(1)} async-done(((f32[16,1,512]{2,1,0:T(1,128)}), f32[16,1,512]{2,1,0:T(1,128)S(1)}, u32[]{:S(2)}, u32[]{:S(2)}) %all-to-all-start.5) | async-done | bytes 32800 | tf_op jit(solution)/shard_map/all_to_all | solution.py:36
  64.2 3.7 %all-to-all-start.4 = ((f32[16,1,512]{2,1,0:T(1,128)}), f32[16,1,512]{2,1,0:T(1,128)S(1)}, u32[]{:S(2)}, u32[]{:S(2)}) async-start(f32[16,1,512]{2,1,0:T(1,128)} %reshape.181), calls=%async_computation.4 | async-start | bytes 65536 | tf_op jit(solution)/shard_map/all_to_all | solution.py:36
  68.8 6.7 %all-to-all-done.4 = f32[16,1,512]{2,1,0:T(1,128)S(1)} async-done(((f32[16,1,512]{2,1,0:T(1,128)}), f32[16,1,512]{2,1,0:T(1,128)S(1)}, u32[]{:S(2)}, u32[]{:S(2)}) %all-to-all-start.4) | async-done | bytes 32800 | tf_op jit(solution)/shard_map/all_to_all | solution.py:36
  75.5 3.7 %all-to-all-start.6 = ((f32[16,16,256]{2,1,0:T(8,128)}), f32[16,16,256]{2,1,0:T(8,128)S(1)}, u32[]{:S(2)}, u32[]{:S(2)}) async-start(f32[16,16,256]{2,1,0:T(8,128)} %fusion.6), calls=%async_computation.6 | async-start | bytes 524288 | tf_op jit(solution)/shard_map/all_to_all | solution.py:36
  80.3 11.0 %all-to-all-done.6 = f32[16,16,256]{2,1,0:T(8,128)S(1)} async-done(((f32[16,16,256]{2,1,0:T(8,128)}), f32[16,16,256]{2,1,0:T(8,128)S(1)}, u32[]{:S(2)}, u32[]{:S(2)}) %all-to-all-start.6) | async-done | bytes 262176 | tf_op jit(solution)/shard_map/all_to_all | solution.py:36
  91.2 3.7 %all-to-all-start.3 = ((f32[16,16,256]{2,1,0:T(8,128)}), f32[16,16,256]{2,1,0:T(8,128)S(1)}, u32[]{:S(2)}, u32[]{:S(2)}) async-start(f32[16,16,256]{2,1,0:T(8,128)} %fusion.8), calls=%async_computation.3 | async-start | bytes 524288 | tf_op jit(solution)/shard_map/all_to_all | solution.py:36
  97.0 8.6 %all-to-all-done.3 = f32[16,16,256]{2,1,0:T(8,128)S(1)} async-done(((f32[16,16,256]{2,1,0:T(8,128)}), f32[16,16,256]{2,1,0:T(8,128)S(1)}, u32[]{:S(2)}, u32[]{:S(2)}) %all-to-all-start.3) | async-done | bytes 262176 | tf_op jit(solution)/shard_map/all_to_all | solution.py:36
  105.6 3.7 %all-to-all-start.7 = ((f32[16,16,512]{2,1,0:T(8,128)}), f32[16,16,512]{2,1,0:T(8,128)S(1)}, u32[]{:S(2)}, u32[]{:S(2)}) async-start(f32[16,16,512]{2,1,0:T(8,128)} %fusion.2), calls=%async_computation.7 | async-start | bytes 1048576 | tf_op jit(solution)/shard_map/all_to_all | solution.py:36
  112.8 12.8 %all-to-all-done.7 = f32[16,16,512]{2,1,0:T(8,128)S(1)} async-done(((f32[16,16,512]{2,1,0:T(8,128)}), f32[16,16,512]{2,1,0:T(8,128)S(1)}, u32[]{:S(2)}, u32[]{:S(2)}) %all-to-all-start.7) | async-done | bytes 524320 | tf_op jit(solution)/shard_map/all_to_all | solution.py:36
  125.6 3.7 %all-to-all-start.2 = ((f32[16,16,512]{2,1,0:T(8,128)}), f32[16,16,512]{2,1,0:T(8,128)S(1)}, u32[]{:S(2)}, u32[]{:S(2)}) async-start(f32[16,16,512]{2,1,0:T(8,128)} %fusion.4), calls=%async_computation.2 | async-start | bytes 1048576 | tf_op jit(solution)/shard_map/all_to_all | solution.py:36
  132.0 14.0 %all-to-all-done.2 = f32[16,16,512]{2,1,0:T(8,128)S(1)} async-done(((f32[16,16,512]{2,1,0:T(8,128)}), f32[16,16,512]{2,1,0:T(8,128)S(1)}, u32[]{:S(2)}, u32[]{:S(2)}) %all-to-all-start.2) | async-done | bytes 524320 | tf_op jit(solution)/shard_map/all_to_all | solution.py:36
  146.1 14.5 %all_to_all.70 = bf16[16,16,512]{2,1,0:T(8,128)(2,1)S(1)} all-to-all(bf16[16,16,512]{2,1,0:T(8,128)(2,1)S(1)} %broadcast_in_dim.9), channel_id=1, replica_groups=mesh['grp'=2,'kv'=16,'tp'=8] {'kv'}, dimensions={0} | all-to-all | bytes 524288 | tf_op jit(solution)/shard_map/all_to_all | solution.py:13
  161.9 11.9 %all_to_all.71 = bf16[8,256,32]{1,2,0:T(8,128)(2,1)S(1)} all-to-all(bf16[8,256,32]{1,2,0:T(8,128)(2,1)S(1)} %bitcast.64), channel_id=1, replica_groups=mesh['grp'=2,'kv'=16,'tp'=8] {'tp'}, dimensions={0} | all-to-all | bytes 262144 | tf_op jit(solution)/shard_map/all_to_all | solution.py:42
  178.9 7.6 %all-to-all-done.10 = bf16[8,256,32]{1,2,0:T(8,128)(2,1)S(1)} async-done(((bf16[8,256,32]{1,2,0:T(8,128)(2,1)}), bf16[8,256,32]{1,2,0:T(8,128)(2,1)S(1)}, u32[]{:S(2)}, u32[]{:S(2)}) %all-to-all-start.10) | async-done | bytes 131104 | tf_op jit(solution)/shard_map/all_to_all | solution.py:13
  192.8 12.1 %all_to_all.72 = f32[16,1,256]{2,1,0:T(1,128)S(1)} all-to-all(f32[16,1,256]{2,1,0:T(1,128)S(1)} %broadcast_in_dim.11), channel_id=1, replica_groups=mesh['grp'=2,'kv'=16,'tp'=8] {'kv'}, dimensions={0} | all-to-all | bytes 32768 | tf_op jit(solution)/shard_map/all_to_all | solution.py:13
  205.0 46.0 %reduce-scatter.4.cloned.1.call-done = f32[88,512]{1,0:T(8,128)} async-done(((f32[1408,512]{1,0:T(8,128)}), f32[88,512]{1,0:T(8,128)}) %reduce-scatter.4.cloned.1.call-update) | async-done | bytes 180240
  252.0 19.5 %all_gather.3 = bf16[256,1408]{0,1:T(8,128)(2,1)S(1)} all-gather(bf16[256,88]{0,1:T(8,128)(2,1)S(1)} %fusion.11), channel_id=1, replica_groups=mesh['grp'=2,'kv'=16,'tp'=8] {'kv'}, dimensions={1}, use_global_device_ids=true | all-gather | bytes 765952 | tf_op jit(solution)/shard_map/all_gather | solution.py:133
  272.5 6.4 %all-to-all-start.12 = ((bf16[8,256,32]{1,2,0:T(8,128)(2,1)}), bf16[8,256,32]{1,2,0:T(8,128)(2,1)S(1)}, u32[]{:S(2)}, u32[]{:S(2)}) async-start(bf16[8,256,32]{1,2,0:T(8,128)(2,1)} %bitcast.18), calls=%async_computation.12 | async-start | bytes 262144 | tf_op jit(solution)/shard_map/all_to_all | solution.py:42
  279.6 7.7 %all-to-all-done.12 = bf16[8,256,32]{1,2,0:T(8,128)(2,1)S(1)} async-done(((bf16[8,256,32]{1,2,0:T(8,128)(2,1)}), bf16[8,256,32]{1,2,0:T(8,128)(2,1)S(1)}, u32[]{:S(2)}, u32[]{:S(2)}) %all-to-all-start.12) | async-done | bytes 131104 | tf_op jit(solution)/shard_map/all_to_all | solution.py:42
  (91 shorter events, 31.5 us)
Async XLA Ops:
  7.2 179.4 %copy-start = (bf16[256,1408]{1,0:T(8,128)(2,1)S(1)}, bf16[256,1408]{1,0:T(8,128)(2,1)}, u32[]{:S(2)}) copy-start(bf16[256,1408]{1,0:T(8,128)(2,1)} %param.30) | copy-start | bytes 2162692
  7.2 39.2 %copy-start.8 = (bf16[256,32]{0,1:T(8,128)(2,1)S(1)}, bf16[256,32]{0,1:T(8,128)(2,1)}, u32[]{:S(2)}) copy-start(bf16[256,32]{0,1:T(8,128)(2,1)} %param.22) | copy-start | bytes 49156
  8.7 15.8 %all-to-all-start = ((bf16[8,256,32]{1,2,0:T(8,128)(2,1)}), bf16[8,256,32]{1,2,0:T(8,128)(2,1)S(1)}, u32[]{:S(2)}, u32[]{:S(2)}) async-start(bf16[8,256,32]{1,2,0:T(8,128)(2,1)} %broadcast_in_dim.8), calls=%async_computation | async-start | bytes 262144 | tf_op jit(solution)/shard_map/all_to_all | solution.py:13
  16.5 40.1 %copy-start.9 = (bf16[256,32]{0,1:T(8,128)(2,1)S(1)}, bf16[256,32]{0,1:T(8,128)(2,1)}, u32[]{:S(2)}) copy-start(bf16[256,32]{0,1:T(8,128)(2,1)} %param.23) | copy-start | bytes 49156
  25.2 27.4 %all-to-all-start.1 = ((f32[16,1,16]{2,1,0:T(1,128)}), f32[16,1,16]{2,1,0:T(1,128)S(1)}, u32[]{:S(2)}, u32[]{:S(2)}) async-start(f32[16,1,16]{2,1,0:T(1,128)} %all_to_all.44), calls=%async_computation.1 | async-start | bytes 16384 | tf_op jit(solution)/shard_map/all_to_all | solution.py:36
  45.5 22.4 %copy-start.5 = (bf16[256,256]{1,0:T(8,128)(2,1)S(1)}, bf16[256,256]{1,0:T(8,128)(2,1)}, u32[]{:S(2)}) copy-start(bf16[256,256]{1,0:T(8,128)(2,1)} %param.19) | copy-start | bytes 393220
  46.0 33.3 %copy-start.10 = (f32[16,4]{0,1:T(4,128)S(1)}, f32[16,4]{0,1:T(4,128)}, u32[]{:S(2)}) copy-start(f32[16,4]{0,1:T(4,128)} %param.26) | copy-start | bytes 772
  46.0 33.4 %copy-start.6 = (bf16[256,256]{1,0:T(8,128)(2,1)S(1)}, bf16[256,256]{1,0:T(8,128)(2,1)}, u32[]{:S(2)}) copy-start(bf16[256,256]{1,0:T(8,128)(2,1)} %param.18) | copy-start | bytes 393220
  46.0 49.0 %copy-start.3 = (bf16[256,512]{1,0:T(8,128)(2,1)S(1)}, bf16[256,512]{1,0:T(8,128)(2,1)}, u32[]{:S(2)}) copy-start(bf16[256,512]{1,0:T(8,128)(2,1)} %param.20) | copy-start | bytes 786436
  46.4 49.6 %copy-start.4 = (bf16[256,512]{1,0:T(8,128)(2,1)S(1)}, bf16[256,512]{1,0:T(8,128)(2,1)}, u32[]{:S(2)}) copy-start(bf16[256,512]{1,0:T(8,128)(2,1)} %param.21) | copy-start | bytes 786436
  52.6 11.6 %all-to-all-start.5 = ((f32[16,1,512]{2,1,0:T(1,128)}), f32[16,1,512]{2,1,0:T(1,128)S(1)}, u32[]{:S(2)}, u32[]{:S(2)}) async-start(f32[16,1,512]{2,1,0:T(1,128)} %reshape.179), calls=%async_computation.5 | async-start | bytes 65536 | tf_op jit(solution)/shard_map/all_to_all | solution.py:36
  64.2 11.3 %all-to-all-start.4 = ((f32[16,1,512]{2,1,0:T(1,128)}), f32[16,1,512]{2,1,0:T(1,128)S(1)}, u32[]{:S(2)}, u32[]{:S(2)}) async-start(f32[16,1,512]{2,1,0:T(1,128)} %reshape.181), calls=%async_computation.4 | async-start | bytes 65536 | tf_op jit(solution)/shard_map/all_to_all | solution.py:36
  75.5 15.7 %all-to-all-start.6 = ((f32[16,16,256]{2,1,0:T(8,128)}), f32[16,16,256]{2,1,0:T(8,128)S(1)}, u32[]{:S(2)}, u32[]{:S(2)}) async-start(f32[16,16,256]{2,1,0:T(8,128)} %fusion.6), calls=%async_computation.6 | async-start | bytes 524288 | tf_op jit(solution)/shard_map/all_to_all | solution.py:36
  91.2 14.4 %all-to-all-start.3 = ((f32[16,16,256]{2,1,0:T(8,128)}), f32[16,16,256]{2,1,0:T(8,128)S(1)}, u32[]{:S(2)}, u32[]{:S(2)}) async-start(f32[16,16,256]{2,1,0:T(8,128)} %fusion.8), calls=%async_computation.3 | async-start | bytes 524288 | tf_op jit(solution)/shard_map/all_to_all | solution.py:36
  95.0 17.0 %copy-start.7 = (f32[16,4,64]{2,1,0:T(4,128)S(1)}, f32[16,4,64]{2,1,0:T(4,128)}, u32[]{:S(2)}) copy-start(f32[16,4,64]{2,1,0:T(4,128)} %param.25) | copy-start | bytes 49156
  105.6 20.0 %all-to-all-start.7 = ((f32[16,16,512]{2,1,0:T(8,128)}), f32[16,16,512]{2,1,0:T(8,128)S(1)}, u32[]{:S(2)}, u32[]{:S(2)}) async-start(f32[16,16,512]{2,1,0:T(8,128)} %fusion.2), calls=%async_computation.7 | async-start | bytes 1048576 | tf_op jit(solution)/shard_map/all_to_all | solution.py:36
  125.6 20.4 %all-to-all-start.2 = ((f32[16,16,512]{2,1,0:T(8,128)}), f32[16,16,512]{2,1,0:T(8,128)S(1)}, u32[]{:S(2)}, u32[]{:S(2)}) async-start(f32[16,16,512]{2,1,0:T(8,128)} %fusion.4), calls=%async_computation.2 | async-start | bytes 1048576 | tf_op jit(solution)/shard_map/all_to_all | solution.py:36
  131.5 30.4 %copy-start.1 = (f32[16,4,64,128]{3,2,1,0:T(8,128)}, f32[16,4,64,128]{3,2,1,0:T(8,128)S(1)}, u32[]{:S(2)}) copy-start(f32[16,4,64,128]{3,2,1,0:T(8,128)S(1)} %multiply_add_fusion) | copy-start | bytes 6291460
  131.5 47.4 %copy-start.12 = (bf16[256]{0:T(256)(128)(2,1)S(1)}, bf16[256]{0:T(256)(128)(2,1)}, u32[]{:S(2)}) copy-start(bf16[256]{0:T(256)(128)(2,1)} %param.28) | copy-start | bytes 1540
  160.6 26.4 %copy-start.2 = (bf16[256,1408]{1,0:T(8,128)(2,1)S(1)}, bf16[256,1408]{1,0:T(8,128)(2,1)}, u32[]{:S(2)}) copy-start(bf16[256,1408]{1,0:T(8,128)(2,1)} %param.29) | copy-start | bytes 2162692
  175.2 11.2 %all-to-all-start.10 = ((bf16[8,256,32]{1,2,0:T(8,128)(2,1)}), bf16[8,256,32]{1,2,0:T(8,128)(2,1)S(1)}, u32[]{:S(2)}, u32[]{:S(2)}) async-start(bf16[8,256,32]{1,2,0:T(8,128)(2,1)} %broadcast_in_dim.10), calls=%async_computation.10 | async-start | bytes 262144 | tf_op jit(solution)/shard_map/all_to_all | solution.py:13
  178.8 72.2 %reduce-scatter.4.cloned.1.call-start = ((), (), s32[]{:S(2)}) async-start(), calls=%async_computation.14 | async-start | bytes 3063808
  192.7 78.8 %copy-start.11 = (bf16[1408,256]{1,0:T(8,128)(2,1)S(1)}, bf16[1408,256]{1,0:T(8,128)(2,1)}, u32[]{:S(2)}) copy-start(bf16[1408,256]{1,0:T(8,128)(2,1)} %param.31) | copy-start | bytes 2162692
  272.5 14.8 %all-to-all-start.12 = ((bf16[8,256,32]{1,2,0:T(8,128)(2,1)}), bf16[8,256,32]{1,2,0:T(8,128)(2,1)S(1)}, u32[]{:S(2)}, u32[]{:S(2)}) async-start(bf16[8,256,32]{1,2,0:T(8,128)(2,1)} %bitcast.18), calls=%async_computation.12 | async-start | bytes 262144 | tf_op jit(solution)/shard_map/all_to_all | solution.py:42
Sparse Core Ops, SparseCore 0:
  192.9 58.0 reduce-scatter.3
where the time goes:
time: 296 us; the launch traced here: 295 us
  waiting for transfers between devices  134 us (45%)
  starting transfers between devices  60.8 us (21%)
  blocking collectives  58 us (20%)
  between operations  14.4 us (5%)
  local copies, waits for them, and re-layouts  10.2 us (3%)
  other arithmetic  9.97 us (3%)
  matrix products  7.66 us (3%)
    all_to_all x7, waiting for transfers between devices, summed_on_arrival(): pieces = lax.all_to_all(split_up(array, dim, count), axis, 0, 0, tiled=True)  65.2 us
    unnamed x2, waiting for transfers between devices  46 us
    all_to_all x7, starting transfers between devices, summed_on_arrival(): pieces = lax.all_to_all(split_up(array, dim, count), axis, 0, 0, tiled=True)  42.9 us
    all_to_all x2, blocking collectives, copy_for_each(): lax.all_to_all(jnp.broadcast_to(array[None], (count, *array.shape)), axis...  26.6 us
    all_gather x1, blocking collectives, shards(): lax.all_gather(hidden_share, 'kv', axis=1, tiled=True)  19.5 us
    all_to_all x2, waiting for transfers between devices, copy_for_each(): lax.all_to_all(jnp.broadcast_to(array[None], (count, *array.shape)), axis...  14.8 us
    all_to_all x1, blocking collectives, sum_at_owner(): pieces = lax.all_to_all(split_up(array, dim, count), axis, 0, 0, tiled=True)  11.9 us
    all_to_all x2, starting transfers between devices, copy_for_each(): lax.all_to_all(jnp.broadcast_to(array[None], (count, *array.shape)), axis...  11.4 us
  transfers between devices with their start and end apart: 11, of which 11 were waited for; matrix products, arithmetic and copies ran while one was open for 5% of the time, Pallas kernels for 0%

commit v1 on v0

v1 whole, which is shorter than its diff:
```python
import jax
import jax.numpy as jnp
from jax import lax
from jax.sharding import Mesh, PartitionSpec as P

DQK = 64
DV = 128
CORES = 2
LANES = 128
BF = jnp.bfloat16
F32 = jnp.float32


def swapped(array):
    return lax.ppermute(array, "c", [(0, 1), (1, 0)])


def spread(array, axes, count):
    return lax.all_to_all(
        jnp.broadcast_to(array[None], (count, *array.shape)), axes, 0, 0, tiled=True
    )


def exchanged(pieces, axes):
    return lax.all_to_all(pieces, axes, 0, 0, tiled=True)


def tdot(left_t, right):
    return lax.dot_general(left_t, right, (((0,), (0,)), ((), ())), preferred_element_type=F32)


def dot_t(weight, rows):
    return lax.dot_general(weight, rows, (((0,), (1,)), ((), ())), preferred_element_type=F32)


def two_parts(values):
    high = values.astype(BF)
    return high, (values - high.astype(F32)).astype(BF)


def padded(array, width):
    return jnp.pad(array, ((0, 0), (0, width - array.shape[1])))


def shards(
    tokens,
    norm_gain,
    w_query,
    w_key,
    w_value,
    w_outgate,
    w_input_gate,
    w_forget_gate,
    memory,
    normalizer,
    stabilizer,
    w_mix_out,
    ffn_gain,
    w_gate,
    w_up,
    w_down,
):
    ny, nx = lax.axis_size("y"), lax.axis_size("x")
    core, at_x = lax.axis_index("c"), lax.axis_index("x")
    seqs, feats = tokens.shape
    own, heads = memory.shape[:2]
    half = seqs // CORES
    rows = nx * feats
    width = CORES * ny * rows

    w_in = lax.dynamic_slice_in_dim(w_input_gate, at_x * heads, heads, 1)
    w_fg = lax.dynamic_slice_in_dim(w_forget_gate, at_x * heads, heads, 1)
    gates = padded(jnp.concatenate([w_in, w_fg], axis=1), LANES)
    w_first = jnp.concatenate([w_query, w_key, w_value, w_outgate, gates], axis=1)
    w_first_o = swapped(w_first)
    gains = jnp.stack([norm_gain, ffn_gain])
    gains_o = swapped(gains).astype(F32)
    gains = gains.astype(F32)
    w_mix_o = swapped(w_mix_out)
    w_gate_o = swapped(w_gate)
    w_up_o = swapped(w_up)
    w_down_o = swapped(w_down)

    turned = tokens.T.reshape(feats, ny, CORES, own).transpose(2, 0, 1, 3)
    turned = turned.reshape(CORES, 1, feats, half)
    sent = jnp.broadcast_to(turned, (CORES, nx, feats, half)).reshape(-1, feats, half)
    wide = exchanged(sent, ("c", "x")).reshape(CORES, rows, half)
    mine = lax.dynamic_index_in_dim(wide, core, 0, keepdims=False)
    other = lax.dynamic_index_in_dim(wide, 1 - core, 0, keepdims=False)

    def products(pair, at, ours, theirs):
        first = (pair[0].astype(F32) * gains[at][:, None]).astype(BF)
        second = (pair[1].astype(F32) * gains_o[at][:, None]).astype(BF)
        return tdot(first, ours) + tdot(second, theirs)

    def squares(pair):
        return sum(jnp.sum(jnp.square(p.astype(F32)), axis=0) for p in pair)[:, None]

    z = products((mine, other), 0, w_first, w_first_o)
    main = z.shape[1] - LANES
    small = jnp.concatenate([z[:, main : main + 2 * heads], squares((mine, other))], axis=1)
    extra = padded(jnp.concatenate(two_parts(small), axis=1), LANES)
    sent = jnp.concatenate([z[:, :main].astype(BF), extra], axis=1).reshape(ny, own, -1)
    z = jnp.sum(exchanged(sent, "y").astype(F32), axis=0)
    each = 2 * heads + 1
    small = z[:, main : main + each] + z[:, main + each : main + 2 * each]
    scale1 = lax.rsqrt(small[:, 2 * heads :] / width + 1e-06)
    z = scale1 * z[:, :main]
    nq, nv = heads * DQK, heads * DV
    query = z[:, :nq].reshape(own, heads, DQK) * DQK ** (-0.5)
    key = z[:, nq : 2 * nq].reshape(own, heads, DQK)
    value = z[:, 2 * nq : 2 * nq + nv].reshape(own, heads, DV)
    outgate = z[:, 2 * nq + nv :]
    igate = scale1 * small[:, :heads]
    lforget = jax.nn.log_sigmoid(scale1 * small[:, heads : 2 * heads])
    new_stabilizer = jnp.maximum(lforget + stabilizer, igate)
    decay = jnp.exp(lforget + stabilizer - new_stabilizer)
    inflow = jnp.exp(igate - new_stabilizer)
    new_memory = (
        decay[:, :, None, None] * memory
        + inflow[:, :, None, None] * key[:, :, :, None] * value[:, :, None, :]
    )
    new_normalizer = decay[:, :, None] * normalizer + inflow[:, :, None] * key
    numer = jnp.einsum("bhd,bhde->bhe", query, new_memory)
    denom = jnp.sum(query * new_normalizer, axis=-1)
    readout = numer / jnp.maximum(jnp.abs(denom), jnp.exp(-new_stabilizer))[:, :, None]
    gated = (jax.nn.sigmoid(outgate) * readout.reshape(own, nv)).astype(BF)

    gated = spread(gated, "y", ny).reshape(half, nv)
    partial = jnp.stack([dot_t(w_mix_out, gated), dot_t(w_mix_o, gated)]).astype(BF)
    sent = partial.reshape(CORES, nx, feats, half).transpose(1, 0, 2, 3)
    total = jnp.sum(exchanged(sent, "x").astype(F32), axis=0)
    skip = jnp.stack([mine, other]).reshape(CORES, nx, feats, half)
    skip = lax.dynamic_index_in_dim(skip, at_x, 1, keepdims=False)
    mixed_in = (skip.astype(F32) + total).astype(BF)
    mixed_o = swapped(mixed_in[1])

    wide = spread(mixed_in, "x", nx)
    pair = (wide[:, 0].reshape(rows, half), wide[:, 1].reshape(rows, half))
    gate = products(pair, 1, w_gate, w_gate_o)
    up = products(pair, 1, w_up, w_up_o)
    extra = padded(jnp.concatenate(two_parts(squares(pair)), axis=1), LANES)
    sent = jnp.concatenate([gate.astype(BF), up.astype(BF), extra], axis=1).reshape(ny, own, -1)
    z = jnp.sum(exchanged(sent, "y").astype(F32), axis=0)
    ff = gate.shape[1]
    scale2 = lax.rsqrt((z[:, 2 * ff : 2 * ff + 1] + z[:, 2 * ff + 1 : 2 * ff + 2]) / width + 1e-06)
    hidden = (jax.nn.silu(scale2 * z[:, :ff]) * (scale2 * z[:, ff : 2 * ff])).astype(BF)

    hidden = spread(hidden, "y", ny).reshape(half, ff)
    ours, theirs = dot_t(w_down, hidden).astype(BF), dot_t(w_down_o, hidden).astype(BF)
    first = core == 0
    partial = jnp.stack([jnp.where(first, ours, theirs), jnp.where(first, theirs, ours)])
    got = exchanged(partial.reshape(CORES * nx, feats, half), ("c", "x"))
    total = jnp.sum(got.reshape(CORES, nx, feats, half).astype(F32), axis=1)
    kept = mixed_in[0]
    skip = jnp.stack([jnp.where(first, kept, mixed_o), jnp.where(first, mixed_o, kept)])
    out = (skip.astype(F32) + total).astype(BF).reshape(CORES, feats, ny, own)
    layer_out = out.transpose(1, 2, 0, 3).reshape(feats, seqs).T
    return (layer_out, new_memory, new_normalizer, new_stabilizer)


def solution(mesh):
    sizes = mesh.shape
    shape = (sizes["grp"], sizes["kv"] // CORES, CORES, sizes["tp"])
    fine = Mesh(mesh.devices.reshape(shape), ("grp", "y", "c", "x"))
    kv, tp = ("y", "c"), "x"
    every = P("grp", ("y", "c", "x"))
    in_specs = (
        every,
        P(kv),
        P(kv, tp),
        P(kv, tp),
        P(kv, tp),
        P(kv, tp),
        P(kv, None),
        P(kv, None),
        P(("grp", *kv), tp, None, None),
        P(("grp", *kv), tp, None),
        P(("grp", *kv), tp),
        P(tp, kv),
        P(kv),
        P(kv, tp),
        P(kv, tp),
        P(tp, kv),
    )
    out_specs = (
        every,
        P(("grp", *kv), tp, None, None),
        P(("grp", *kv), tp, None),
        P(("grp", *kv), tp),
    )
    return jax.shard_map(shards, mesh=fine, in_specs=in_specs, out_specs=out_specs, check_vma=False)
```

time: 296 us -> 159 us (0.54)
  waiting for transfers between devices: 134 us -> 42.1 us
  blocking collectives: 58 us -> 19.4 us
  between operations: 14.4 us -> 1.17 us
  starting transfers between devices: 60.8 us -> 71.3 us
  matrix products: 7.66 us -> 3.29 us
  local copies, waits for them, and re-layouts: 10.2 us -> 13.7 us
    all_to_all x10 -> x7, waiting for transfers between devices: 87.7 us -> 40.1 us  [the longest x4 27.3 us: exchanged(): return lax.all_to_all(pieces, axes, 0, 0, tiled=True)]
    unnamed x2 -> x0, waiting for transfers between devices: 46 us -> none
    all_gather x1 -> x0, blocking collectives: 19.5 us -> none  [shards(): lax.all_gather(hidden_share, 'kv', axis=1, tiled=True)]
    all_to_all x3 -> x1, blocking collectives: 38.5 us -> 19.4 us  [exchanged(): return lax.all_to_all(pieces, axes, 0, 0, tiled=True)]
    ppermute x0 -> x7, starting transfers between devices: none -> 14 us  [swapped(): return lax.ppermute(array, 'c', [(0, 1), (1, 0)])]
    dot_general x10, matrix products: 7.28 us -> 2.91 us  [the longest x6 1.99 us: tdot(): lax.dot_general(left_t, right, (((0,), (0,)), ((), ())), preferred_elemen...]
    all_to_all x10 -> x7, starting transfers between devices: 60.7 us -> 57.3 us  [the longest x4 46.5 us: exchanged(): return lax.all_to_all(pieces, axes, 0, 0, tiled=True)]
    unnamed x33 -> x31, local copies, waits for them, and re-layouts: 5.94 us -> 6.22 us
  transfers between devices with their start and end apart: 11 -> 14, of which waited for: 11 -> 8; matrix products, arithmetic and copies ran while one was open for 5% -> 6% of each run, Pallas kernels for 0% -> 0%
where the time goes in v1:
time: 159 us; the launch traced here: 158 us
  starting transfers between devices  71.3 us (45%)
  waiting for transfers between devices  42.1 us (26%)
  blocking collectives  19.4 us (12%)
  local copies, waits for them, and re-layouts  13.7 us (9%)
  other arithmetic  7.06 us (4%)
  matrix products  3.29 us (2%)
    all_to_all x4, starting transfers between devices, exchanged(): return lax.all_to_all(pieces, axes, 0, 0, tiled=True)  46.5 us
    all_to_all x4, waiting for transfers between devices, exchanged(): return lax.all_to_all(pieces, axes, 0, 0, tiled=True)  27.3 us
    all_to_all x1, blocking collectives, exchanged(): return lax.all_to_all(pieces, axes, 0, 0, tiled=True)  19.4 us
    ppermute x7, starting transfers between devices, swapped(): return lax.ppermute(array, 'c', [(0, 1), (1, 0)])  14 us
    all_to_all x3, waiting for transfers between devices, spread(): lax.all_to_all(jnp.broadcast_to(array[None], (count, *array.shape)), axes...  12.8 us
    all_to_all x3, starting transfers between devices, spread(): lax.all_to_all(jnp.broadcast_to(array[None], (count, *array.shape)), axes...  10.8 us
    unnamed x31, local copies, waits for them, and re-layouts  6.22 us
  transfers between devices with their start and end apart: 14, of which 8 were waited for; matrix products, arithmetic and copies ran while one was open for 6% of the time, Pallas kernels for 0%

profile of v1, /device:TPU:513, one launch (start us, length us, event | category | flops | bytes accessed | tf_op | source)
XLA Modules:
  0.0 158.0 jit_solution(12133836274309594470)
XLA Ops:
  2.3 23.9 %all-to-all-start = ((bf16[16,32,128]{2,1,0:T(8,128)(2,1)}), bf16[16,32,128]{2,1,0:T(8,128)(2,1)S(1)}, u32[]{:S(2)}, u32[]{:S(2)}) async-start(bf16[16,32,128]{2,1,0:T(8,128)(2,1)} %bitcast.4), calls=%async_computation | async-start | bytes 262144 | tf_op jit(solution)/shard_map/all_to_all | solution.py:25
  26.1 0.9 constant_dynamic-update-slice_fusion.3
  27.9 0.9 constant_dynamic-update-slice_fusion.2
  28.8 1.0 constant_dynamic-update-slice_fusion.1
  29.8 1.0 constant_dynamic-update-slice_fusion
  31.7 1.8 %collective-permute-done = bf16[2,256]{1,0:T(2,128)(2,1)S(1)} collective-permute-done((bf16[2,256]{1,0:T(2,128)(2,1)S(1)}, bf16[2,256]{1,0:T(2,128)(2,1)S(1)}, u32[]{:S(2)}, u32[]{:S(2)}) %collective-permute-start) | collective-permute-done | bytes 1056 | tf_op jit(solution)/shard_map/ppermute | solution.py:15
  35.5 3.7 %all-to-all-start.1 = ((bf16[8,16,1664]{2,1,0:T(8,128)(2,1)}), bf16[8,16,1664]{2,1,0:T(8,128)(2,1)S(1)}, u32[]{:S(2)}, u32[]{:S(2)}) async-start(bf16[8,16,1664]{2,1,0:T(8,128)(2,1)} %bitcast.15), calls=%async_computation.1 | async-start | bytes 851968 | tf_op jit(solution)/shard_map/all_to_all | solution.py:25
  39.3 14.3 %all-to-all-done.1 = bf16[8,16,1664]{2,1,0:T(8,128)(2,1)S(1)} async-done(((bf16[8,16,1664]{2,1,0:T(8,128)(2,1)}), bf16[8,16,1664]{2,1,0:T(8,128)(2,1)S(1)}, u32[]{:S(2)}, u32[]{:S(2)}) %all-to-all-start.1) | async-done | bytes 426016 | tf_op jit(solution)/shard_map/all_to_all | solution.py:25
  55.3 2.0 %multiply_add_fusion = f32[16,4,64,128]{3,2,1,0:T(8,128)S(1)} fusion(f32[16,4,64,128]{3,2,1,0:T(8,128)} %param.24, f32[16,4,128]{2,1,0:T(4,128)S(1)} %mul.183, f32[16,4,64]{2,1,0:T(4,128)S(1)} %get-tuple-element.24, f32[16,4]{1,0:T(8,128)S(1)} %get-tuple-element.25), kind=kLoop, calls=%fused_computation.5 | loop fusion | flops 1572864 | bytes 4243712 | tf_op jit(solution)/shard_map/add | solution.py:120
  58.5 3.6 %all-to-all-start.2 = ((bf16[8,16,512]{2,1,0:T(8,128)(2,1)}), bf16[8,16,512]{2,1,0:T(8,128)(2,1)S(1)}, u32[]{:S(2)}, u32[]{:S(2)}) async-start(bf16[8,16,512]{2,1,0:T(8,128)(2,1)} %broadcast_in_dim.12), calls=%async_computation.2 | async-start | bytes 262144 | tf_op jit(solution)/shard_map/all_to_all | solution.py:19
  62.1 1.8 %collective-permute-start.2 = (bf16[512,256]{1,0:T(8,128)(2,1)S(1)}, bf16[512,256]{1,0:T(8,128)(2,1)S(1)}, u32[]{:S(2)}, u32[]{:S(2)}) collective-permute-start(bf16[512,256]{1,0:T(8,128)(2,1)S(1)} %copy-done.6), channel_id=1, source_target_pairs={{0,8},{8,0},{1,9},{9,1},{2,10},{10,2},{3,11},{11,3},{4,12},{12,4},... | collective-permute-start | bytes 786440 | tf_op jit(solution)/shard_map/ppermute | solution.py:15
  63.8 5.9 %all-to-all-done.2 = bf16[8,16,512]{2,1,0:T(8,128)(2,1)S(1)} async-done(((bf16[8,16,512]{2,1,0:T(8,128)(2,1)}), bf16[8,16,512]{2,1,0:T(8,128)(2,1)S(1)}, u32[]{:S(2)}, u32[]{:S(2)}) %all-to-all-start.2) | async-done | bytes 131104 | tf_op jit(solution)/shard_map/all_to_all | solution.py:19
  71.6 1.0 maximum_bitcast_fusion
  73.2 6.6 %all-to-all-start.3 = ((bf16[8,2,32,128]{3,2,1,0:T(8,128)(2,1)}), bf16[8,2,32,128]{3,2,1,0:T(8,128)(2,1)S(1)}, u32[]{:S(2)}, u32[]{:S(2)}) async-start(bf16[8,2,32,128]{3,2,1,0:T(8,128)(2,1)} %copy.99), calls=%async_computation.3 | async-start | bytes 262144 | tf_op jit(solution)/shard_map/all_to_all | solution.py:25
  80.7 7.1 %all-to-all-done.3 = bf16[8,2,32,128]{3,2,1,0:T(8,128)(2,1)S(1)} async-done(((bf16[8,2,32,128]{3,2,1,0:T(8,128)(2,1)}), bf16[8,2,32,128]{3,2,1,0:T(8,128)(2,1)S(1)}, u32[]{:S(2)}, u32[]{:S(2)}) %all-to-all-start.3) | async-done | bytes 131104 | tf_op jit(solution)/shard_map/all_to_all | solution.py:25
  88.5 3.6 %all-to-all-start.4 = ((bf16[8,2,32,128]{3,2,1,0:T(8,128)(2,1)}), bf16[8,2,32,128]{3,2,1,0:T(8,128)(2,1)S(1)}, u32[]{:S(2)}, u32[]{:S(2)}) async-start(bf16[8,2,32,128]{3,2,1,0:T(8,128)(2,1)} %broadcast_in_dim.13), calls=%async_computation.4 | async-start | bytes 262144 | tf_op jit(solution)/shard_map/all_to_all | solution.py:19
  92.1 4.2 %collective-permute-start.5 = (bf16[256,1408]{1,0:T(8,128)(2,1)S(1)}, bf16[256,1408]{1,0:T(8,128)(2,1)S(1)}, u32[]{:S(2)}, u32[]{:S(2)}) collective-permute-start(bf16[256,1408]{1,0:T(8,128)(2,1)S(1)} %copy-done.1), channel_id=1, source_target_pairs={{0,8},{8,0},{1,9},{9,1},{2,10},{10,2},{3,11},{11,3},{4,12},{12,4},... | collective-permute-start | bytes 2162696 | tf_op jit(solution)/shard_map/ppermute | solution.py:15
  96.4 3.3 %all-to-all-done.4 = bf16[8,2,32,128]{3,2,1,0:T(8,128)(2,1)S(1)} async-done(((bf16[8,2,32,128]{3,2,1,0:T(8,128)(2,1)}), bf16[8,2,32,128]{3,2,1,0:T(8,128)(2,1)S(1)}, u32[]{:S(2)}, u32[]{:S(2)}) %all-to-all-start.4) | async-done | bytes 131104 | tf_op jit(solution)/shard_map/all_to_all | solution.py:19
  101.5 19.4 %all_to_all.40 = bf16[8,16,2944]{2,1,0:T(8,128)(2,1)S(1)} all-to-all(bf16[8,16,2944]{2,1,0:T(8,128)(2,1)S(1)} %bitcast.117), channel_id=1, replica_groups=mesh['grp'=2,'y'=8,'c'=2,'x'=8] {'y'}, dimensions={0} | all-to-all | bytes 1507328 | tf_op jit(solution)/shard_map/all_to_all | solution.py:25
  122.2 3.6 %all-to-all-start.6 = ((bf16[8,16,1408]{2,1,0:T(8,128)(2,1)}), bf16[8,16,1408]{2,1,0:T(8,128)(2,1)S(1)}, u32[]{:S(2)}, u32[]{:S(2)}) async-start(bf16[8,16,1408]{2,1,0:T(8,128)(2,1)} %broadcast_in_dim.14), calls=%async_computation.6 | async-start | bytes 720896 | tf_op jit(solution)/shard_map/all_to_all | solution.py:19
  125.8 6.6 %collective-permute-start.6 = (bf16[1408,256]{1,0:T(8,128)(2,1)S(1)}, bf16[1408,256]{1,0:T(8,128)(2,1)S(1)}, u32[]{:S(2)}, u32[]{:S(2)}) collective-permute-start(bf16[1408,256]{1,0:T(8,128)(2,1)S(1)} %copy-done.3), channel_id=1, source_target_pairs={{0,8},{8,0},{1,9},{9,1},{2,10},{10,2},{3,11},{11,3},{4,12},{12,4},... | collective-permute-start | bytes 2162696 | tf_op jit(solution)/shard_map/ppermute | solution.py:15
  132.5 3.6 %all-to-all-done.6 = bf16[8,16,1408]{2,1,0:T(8,128)(2,1)S(1)} async-done(((bf16[8,16,1408]{2,1,0:T(8,128)(2,1)}), bf16[8,16,1408]{2,1,0:T(8,128)(2,1)S(1)}, u32[]{:S(2)}, u32[]{:S(2)}) %all-to-all-start.6) | async-done | bytes 360480 | tf_op jit(solution)/shard_map/all_to_all | solution.py:19
  137.4 12.4 %all-to-all-start.7 = ((bf16[16,32,128]{2,1,0:T(8,128)(2,1)}), bf16[16,32,128]{2,1,0:T(8,128)(2,1)S(1)}, u32[]{:S(2)}, u32[]{:S(2)}) async-start(bf16[16,32,128]{2,1,0:T(8,128)(2,1)} %bitcast.40), calls=%async_computation.7 | async-start | bytes 262144 | tf_op jit(solution)/shard_map/all_to_all | solution.py:25
  151.4 5.8 %all-to-all-done.7 = bf16[16,32,128]{2,1,0:T(8,128)(2,1)S(1)} async-done(((bf16[16,32,128]{2,1,0:T(8,128)(2,1)}), bf16[16,32,128]{2,1,0:T(8,128)(2,1)S(1)}, u32[]{:S(2)}, u32[]{:S(2)}) %all-to-all-start.7) | async-done | bytes 131104 | tf_op jit(solution)/shard_map/all_to_all | solution.py:25
  (117 shorter events, 18.9 us)
Async XLA Ops:
  0.6 30.8 %copy-start.9 = (bf16[256]{0:T(256)(128)(2,1)S(1)}, bf16[256]{0:T(256)(128)(2,1)}, u32[]{:S(2)}) copy-start(bf16[256]{0:T(256)(128)(2,1)} %param.28) | copy-start | bytes 1540
  0.6 30.8 %copy-start.10 = (bf16[256]{0:T(256)(128)(2,1)S(1)}, bf16[256]{0:T(256)(128)(2,1)}, u32[]{:S(2)}) copy-start(bf16[256]{0:T(256)(128)(2,1)} %param.17) | copy-start | bytes 1540
  2.3 31.2 %all-to-all-start = ((bf16[16,32,128]{2,1,0:T(8,128)(2,1)}), bf16[16,32,128]{2,1,0:T(8,128)(2,1)S(1)}, u32[]{:S(2)}, u32[]{:S(2)}) async-start(bf16[16,32,128]{2,1,0:T(8,128)(2,1)} %bitcast.4), calls=%async_computation | async-start | bytes 262144 | tf_op jit(solution)/shard_map/all_to_all | solution.py:25
  30.8 3.2 %collective-permute-start.1 = (bf16[256,1664]{1,0:T(8,128)(2,1)S(1)}, bf16[256,1664]{1,0:T(8,128)(2,1)S(1)}, u32[]{:S(2)}, u32[]{:S(2)}) collective-permute-start(bf16[256,1664]{1,0:T(8,128)(2,1)S(1)} %pad_dynamic-update-slice_fusion), channel_id=1, source_target_pairs={{0,8},{8,0},{1,9},{9,1},{2,10},{10,2},{3,11},{11,3},{4,12},{12,4},... | collective-permute-start | bytes 2555912 | tf_op jit(solution)/shard_map/ppermute | solution.py:15
  31.5 2.0 %collective-permute-start = (bf16[2,256]{1,0:T(2,128)(2,1)S(1)}, bf16[2,256]{1,0:T(2,128)(2,1)S(1)}, u32[]{:S(2)}, u32[]{:S(2)}) collective-permute-start(bf16[2,256]{1,0:T(2,128)(2,1)S(1)} %pad_maximum_fusion.5), channel_id=1, source_target_pairs={{0,8},{8,0},{1,9},{9,1},{2,10},{10,2},{3,11},{11,3},{4,12},{12,4},... | collective-permute-start | bytes 3080 | tf_op jit(solution)/shard_map/ppermute | solution.py:15
  33.5 0.9 copy-start.4
  34.0 5.2 %copy-start.8 = (f32[16,4]{0,1:T(4,128)S(1)}, f32[16,4]{0,1:T(4,128)}, u32[]{:S(2)}) copy-start(f32[16,4]{0,1:T(4,128)} %param.26) | copy-start | bytes 772
  34.4 20.1 %copy-start.7 = (f32[16,4,64]{2,1,0:T(4,128)S(1)}, f32[16,4,64]{2,1,0:T(4,128)}, u32[]{:S(2)}) copy-start(f32[16,4,64]{2,1,0:T(4,128)} %param.25) | copy-start | bytes 49156
  35.5 18.1 %all-to-all-start.1 = ((bf16[8,16,1664]{2,1,0:T(8,128)(2,1)}), bf16[8,16,1664]{2,1,0:T(8,128)(2,1)S(1)}, u32[]{:S(2)}, u32[]{:S(2)}) async-start(bf16[8,16,1664]{2,1,0:T(8,128)(2,1)} %bitcast.15), calls=%async_computation.1 | async-start | bytes 851968 | tf_op jit(solution)/shard_map/all_to_all | solution.py:25
  57.3 15.9 %copy-start = (f32[16,4,64,128]{3,2,1,0:T(8,128)}, f32[16,4,64,128]{3,2,1,0:T(8,128)S(1)}, u32[]{:S(2)}) copy-start(f32[16,4,64,128]{3,2,1,0:T(8,128)S(1)} %multiply_add_fusion) | copy-start | bytes 6291460
  57.3 4.8 %copy-start.6 = (bf16[512,256]{1,0:T(8,128)(2,1)S(1)}, bf16[512,256]{1,0:T(8,128)(2,1)}, u32[]{:S(2)}) copy-start(bf16[512,256]{1,0:T(8,128)(2,1)} %param.27) | copy-start | bytes 786436
  57.7 34.4 %copy-start.1 = (bf16[256,1408]{1,0:T(8,128)(2,1)S(1)}, bf16[256,1408]{1,0:T(8,128)(2,1)}, u32[]{:S(2)}) copy-start(bf16[256,1408]{1,0:T(8,128)(2,1)} %param.30) | copy-start | bytes 2162692
  58.5 11.3 %all-to-all-start.2 = ((bf16[8,16,512]{2,1,0:T(8,128)(2,1)}), bf16[8,16,512]{2,1,0:T(8,128)(2,1)S(1)}, u32[]{:S(2)}, u32[]{:S(2)}) async-start(bf16[8,16,512]{2,1,0:T(8,128)(2,1)} %broadcast_in_dim.12), calls=%async_computation.2 | async-start | bytes 262144 | tf_op jit(solution)/shard_map/all_to_all | solution.py:19
  62.1 7.9 %collective-permute-start.2 = (bf16[512,256]{1,0:T(8,128)(2,1)S(1)}, bf16[512,256]{1,0:T(8,128)(2,1)S(1)}, u32[]{:S(2)}, u32[]{:S(2)}) collective-permute-start(bf16[512,256]{1,0:T(8,128)(2,1)S(1)} %copy-done.6), channel_id=1, source_target_pairs={{0,8},{8,0},{1,9},{9,1},{2,10},{10,2},{3,11},{11,3},{4,12},{12,4},... | collective-permute-start | bytes 786440 | tf_op jit(solution)/shard_map/ppermute | solution.py:15
  71.6 28.9 %copy-start.2 = (bf16[256,1408]{1,0:T(8,128)(2,1)S(1)}, bf16[256,1408]{1,0:T(8,128)(2,1)}, u32[]{:S(2)}) copy-start(bf16[256,1408]{1,0:T(8,128)(2,1)} %param.29) | copy-start | bytes 2162692
  73.2 14.6 %all-to-all-start.3 = ((bf16[8,2,32,128]{3,2,1,0:T(8,128)(2,1)}), bf16[8,2,32,128]{3,2,1,0:T(8,128)(2,1)S(1)}, u32[]{:S(2)}, u32[]{:S(2)}) async-start(bf16[8,2,32,128]{3,2,1,0:T(8,128)(2,1)} %copy.99), calls=%async_computation.3 | async-start | bytes 262144 | tf_op jit(solution)/shard_map/all_to_all | solution.py:25
  88.5 11.3 %all-to-all-start.4 = ((bf16[8,2,32,128]{3,2,1,0:T(8,128)(2,1)}), bf16[8,2,32,128]{3,2,1,0:T(8,128)(2,1)S(1)}, u32[]{:S(2)}, u32[]{:S(2)}) async-start(bf16[8,2,32,128]{3,2,1,0:T(8,128)(2,1)} %broadcast_in_dim.13), calls=%async_computation.4 | async-start | bytes 262144 | tf_op jit(solution)/shard_map/all_to_all | solution.py:19
  92.1 8.7 %collective-permute-start.5 = (bf16[256,1408]{1,0:T(8,128)(2,1)S(1)}, bf16[256,1408]{1,0:T(8,128)(2,1)S(1)}, u32[]{:S(2)}, u32[]{:S(2)}) collective-permute-start(bf16[256,1408]{1,0:T(8,128)(2,1)S(1)} %copy-done.1), channel_id=1, source_target_pairs={{0,8},{8,0},{1,9},{9,1},{2,10},{10,2},{3,11},{11,3},{4,12},{12,4},... | collective-permute-start | bytes 2162696 | tf_op jit(solution)/shard_map/ppermute | solution.py:15
  96.3 4.9 %collective-permute-start.4 = (bf16[256,1408]{1,0:T(8,128)(2,1)}, bf16[256,1408]{1,0:T(8,128)(2,1)S(1)}, u32[]{:S(2)}, u32[]{:S(2)}) collective-permute-start(bf16[256,1408]{1,0:T(8,128)(2,1)} %param.29), channel_id=1, source_target_pairs={{0,8},{8,0},{1,9},{9,1},{2,10},{10,2},{3,11},{11,3},{4,12},{12,4},... | collective-permute-start | bytes 2162696 | tf_op jit(solution)/shard_map/ppermute | solution.py:15
  101.5 24.3 %copy-start.3 = (bf16[1408,256]{1,0:T(8,128)(2,1)S(1)}, bf16[1408,256]{1,0:T(8,128)(2,1)}, u32[]{:S(2)}) copy-start(bf16[1408,256]{1,0:T(8,128)(2,1)} %param.31) | copy-start | bytes 2162692
  122.2 13.9 %all-to-all-start.6 = ((bf16[8,16,1408]{2,1,0:T(8,128)(2,1)}), bf16[8,16,1408]{2,1,0:T(8,128)(2,1)S(1)}, u32[]{:S(2)}, u32[]{:S(2)}) async-start(bf16[8,16,1408]{2,1,0:T(8,128)(2,1)} %broadcast_in_dim.14), calls=%async_computation.6 | async-start | bytes 720896 | tf_op jit(solution)/shard_map/all_to_all | solution.py:19
  125.8 10.5 %collective-permute-start.6 = (bf16[1408,256]{1,0:T(8,128)(2,1)S(1)}, bf16[1408,256]{1,0:T(8,128)(2,1)S(1)}, u32[]{:S(2)}, u32[]{:S(2)}) collective-permute-start(bf16[1408,256]{1,0:T(8,128)(2,1)S(1)} %copy-done.3), channel_id=1, source_target_pairs={{0,8},{8,0},{1,9},{9,1},{2,10},{10,2},{3,11},{11,3},{4,12},{12,4},... | collective-permute-start | bytes 2162696 | tf_op jit(solution)/shard_map/ppermute | solution.py:15
  137.4 19.8 %all-to-all-start.7 = ((bf16[16,32,128]{2,1,0:T(8,128)(2,1)}), bf16[16,32,128]{2,1,0:T(8,128)(2,1)S(1)}, u32[]{:S(2)}, u32[]{:S(2)}) async-start(bf16[16,32,128]{2,1,0:T(8,128)(2,1)} %bitcast.40), calls=%async_computation.7 | async-start | bytes 262144 | tf_op jit(solution)/shard_map/all_to_all | solution.py:25
  149.8 1.3 collective-permute-start.3
  (1 other events, 0.9 us)
